TPU v7x, 32 devices: a whole 2x2x4 slice. The times are simulated.
32 devices in a mesh: ep: 8 (over z, core), tp: 4 (over y, x).
Axes of the slice: x: 2, y: 2, z: 4, core: 2. Of those that a mesh axis runs over, the one named last changes fastest.
Arguments:
- query_vectors: bfloat16 [4096, 4096], P('ep', 'tp'), may hold values from -6 to 6
- key_vectors: bfloat16 [4096, 2048], P('ep', 'tp'), may hold values from -6 to 6
- value_vectors: bfloat16 [4096, 2048], P('ep', 'tp'), may hold values from -64 to 64
- query_gain: float32 [128], replicated, may hold values from 0.1 to 1.9
- key_gain: float32 [128], replicated, may hold values from 0.1 to 1.9
- sink_logits: float32 [32], P('tp'), may hold values from 3 to 7
- moe_rows: bfloat16 [1280, 4096], P('ep', 'tp'), may hold values from -6 to 6
- norm_gain: float32 [4096], replicated, may hold values from 0.1 to 1.9
- expert_ids: int32 [1280, 4], P('ep'), may hold values from 0 to 7, all different within a row; in each aligned block of 160 rows (0 to 159, 160 to 319, ...) at most 120 rows name the same one
- route_weights: float32 [1280, 4], P('ep'), may hold values from 0.25 to 2.5
- expert_gate: bfloat16 [8, 4096, 2048], P('ep', None, 'tp'), may hold values from -0.09375 to 0.09375
- expert_up: bfloat16 [8, 4096, 2048], P('ep', None, 'tp'), may hold values from -0.09375 to 0.09375
- expert_down: bfloat16 [8, 2048, 4096], P('ep', None, 'tp'), may hold values from -0.125 to 0.125
- shared_gate: bfloat16 [4096, 512], P(None, 'tp'), may hold values from -0.09375 to 0.09375
- shared_up: bfloat16 [4096, 512], P(None, 'tp'), may hold values from -0.09375 to 0.09375
- shared_down: bfloat16 [512, 4096], P(None, 'tp'), may hold values from -0.25 to 0.25
Outputs:
- attended: bfloat16 [4096, 4096], P('ep', 'tp')
- moe_out: bfloat16 [1280, 4096], P('ep', 'tp')
Inputs may be any that keep to these rules, and one draw needn't show every extreme that they name: `expert_ids`: each row names 4 different experts. Within the rows of one index of ep (aligned blocks of 160 rows), no expert is named by more than 120 rows, and in some block one expert is named by exactly 120.
All inputs are finite; a program needn't handle non-finite values.
Results may differ from a plain program's by a relative error of at most 0.0071.
Values may be sent and summed in bfloat16 or wider, within the bound.
A program may use at most 128 MiB of HBM per device.

v0:
```python
import jax
import jax.numpy as jnp
from jax import lax
from jax.sharding import PartitionSpec as P

HEAD_DIM = 128
WINDOW = 128
GRID_W = 64
D = 4096
TOP_K = 4
epsilon = 1e-06
rotary_base = 10000.0


def padded_2(block, sides, width):
    for axis, dim in sides:
        count = lax.axis_size(axis)
        forward = [(i, i + 1) for i in range(count - 1)]
        backward = [(target, source) for source, target in forward]
        low = lax.ppermute(
            lax.slice_in_dim(block, block.shape[dim] - width, None, axis=dim), axis, forward
        )
        high = lax.ppermute(lax.slice_in_dim(block, 0, width, axis=dim), axis, backward)
        block = jnp.concatenate([low, block, high], axis=dim)
    return block


def half_turn(halves):
    leading, trailing = jnp.split(halves, 2, axis=-1)
    return jnp.concatenate([-trailing, leading], axis=-1)


def rotate_heads(vectors, head_gain, positions):
    floats = vectors.astype(jnp.float32)
    normed = (
        floats * lax.rsqrt(jnp.mean(floats * floats, axis=-1, keepdims=True) + epsilon) * head_gain
    )
    quarter = HEAD_DIM // 4
    freq_index = jnp.arange(quarter, dtype=jnp.int32).astype(jnp.float32)
    inverse = rotary_base ** (-4.0 * freq_index / HEAD_DIM)
    grid_row = (positions // GRID_W).astype(jnp.float32)[:, None] * inverse
    grid_col = (positions % GRID_W).astype(jnp.float32)[:, None] * inverse
    angles = jnp.concatenate([grid_row, grid_row, grid_col, grid_col], axis=-1)[:, None, :]
    row_half, col_half = jnp.split(normed, 2, axis=-1)
    turned = jnp.concatenate([half_turn(row_half), half_turn(col_half)], axis=-1)
    return (normed * jnp.cos(angles) + turned * jnp.sin(angles)).astype(jnp.bfloat16)


def attend_window(query_vectors, key_vectors, value_vectors, query_gain, key_gain, sink_logits):
    length = query_vectors.shape[0]
    heads_here = sink_logits.shape[0]
    kv_here = key_vectors.shape[1] // HEAD_DIM
    grouping = heads_here // kv_here
    shard_start = lax.axis_index("ep") * length
    positions = shard_start + jnp.arange(length, dtype=jnp.int32)
    queries = rotate_heads(
        query_vectors.reshape(length, heads_here, HEAD_DIM), query_gain, positions
    )
    turned_keys = rotate_heads(key_vectors.reshape(length, kv_here, HEAD_DIM), key_gain, positions)
    turned_keys = turned_keys.reshape(length, kv_here * HEAD_DIM)
    padded = padded_2(jnp.stack([turned_keys, value_vectors]), (("ep", 1),), WINDOW)
    extent = length + 2 * WINDOW
    near_keys = padded[0].reshape(extent, kv_here, HEAD_DIM)
    near_values = padded[1].reshape(extent, kv_here, HEAD_DIM)
    key_pos = shard_start - WINDOW + jnp.arange(extent, dtype=jnp.int32)
    inside = (
        (jnp.abs(positions[:, None] - key_pos[None, :]) <= WINDOW)
        & (key_pos >= 0)[None, :]
        & (key_pos < lax.axis_size("ep") * length)[None, :]
    )
    scores = jnp.einsum(
        "qhgd,khd->hgqk",
        queries.reshape(length, kv_here, grouping, HEAD_DIM),
        near_keys,
        preferred_element_type=jnp.float32,
    ) * HEAD_DIM ** (-0.5)
    raised = jnp.where(inside, jnp.exp(scores), 0.0)
    denominator = jnp.exp(sink_logits).reshape(kv_here, grouping)[:, :, None] + jnp.sum(
        raised, axis=-1
    )
    weights = (raised / denominator[..., None]).astype(jnp.bfloat16)
    mixed = jnp.einsum("hgqk,khd->qhgd", weights, near_values, preferred_element_type=jnp.float32)
    return mixed.astype(jnp.bfloat16).reshape(length, heads_here * HEAD_DIM)


def project(block_rows, gain_piece, gate_rows, up_rows):
    floats = block_rows.astype(jnp.float32)
    weighted = (floats * gain_piece).astype(jnp.bfloat16)
    gate_sum = jnp.dot(weighted, gate_rows, preferred_element_type=jnp.float32)
    up_sum = jnp.dot(weighted, up_rows, preferred_element_type=jnp.float32)
    return (gate_sum, up_sum, jnp.sum(floats * floats, axis=1))


def activate(gate_sum, up_sum, squares):
    factor = lax.rsqrt(squares / D + epsilon)[:, None]
    return (jax.nn.silu(gate_sum * factor) * (up_sum * factor)).astype(jnp.bfloat16)


def shards(
    query_vectors,
    key_vectors,
    value_vectors,
    query_gain,
    key_gain,
    sink_logits,
    moe_rows,
    norm_gain,
    expert_ids,
    route_weights,
    expert_gate,
    expert_up,
    expert_down,
    shared_gate,
    shared_up,
    shared_down,
):
    attended = attend_window(
        query_vectors, key_vectors, value_vectors, query_gain, key_gain, sink_logits
    )
    ep_size = lax.axis_size("ep")
    tokens_here, width_here = moe_rows.shape
    capacity = max(2, 3 * tokens_here * TOP_K // (2 * ep_size))
    slots_all = ep_size * capacity
    flat_ids = expert_ids.reshape(-1)
    onehot = (flat_ids[:, None] == jnp.arange(ep_size, dtype=jnp.int32)[None, :]).astype(jnp.int32)
    slot_index = jnp.sum((jnp.cumsum(onehot, axis=0) - onehot) * onehot, axis=1)
    target = flat_ids * capacity + slot_index
    matches = target[None, :] == jnp.arange(slots_all, dtype=jnp.int32)[:, None]
    present = jnp.any(matches, axis=1)
    owner_row = jnp.arange(tokens_here * TOP_K, dtype=jnp.int32) // TOP_K
    source_row = jnp.sum(jnp.where(matches, owner_row[None, :], 0), axis=1)
    local_gate = expert_gate[0]
    local_up = expert_up[0]
    local_down = expert_down[0]
    units_here = local_gate.shape[1]
    shared_units = shared_gate.shape[1]
    outgoing = jnp.where(
        present[:, None], jnp.take(moe_rows, source_row, axis=0), jnp.zeros((), jnp.bfloat16)
    )
    arrived = lax.all_to_all(
        outgoing.reshape(ep_size, capacity, width_here),
        "ep",
        split_axis=0,
        concat_axis=0,
        tiled=True,
    )
    arrived = arrived.reshape(slots_all, width_here)
    routed = project(
        lax.all_gather(arrived, "tp", axis=1, tiled=True), norm_gain, local_gate, local_up
    )
    shared = project(
        lax.all_gather(moe_rows, "tp", axis=1, tiled=True), norm_gain, shared_gate, shared_up
    )
    gate_sum, up_sum, squares, shared_gsum, shared_usum, own_squares = tuple(
        (new_term for new_term in routed + shared)
    )
    hidden = activate(gate_sum, up_sum, squares)
    shared_hidden = activate(shared_gsum, shared_usum, own_squares)
    packing = units_here // shared_units
    stacked = jnp.concatenate(
        [hidden, shared_hidden.reshape(tokens_here // packing, units_here)], axis=0
    )
    columns = local_down.shape[1]
    portion = lax.all_gather(stacked, "tp", axis=1, tiled=True)
    shards_in = portion.shape[1] // units_here
    routed = jnp.dot(portion[:slots_all], local_down, preferred_element_type=jnp.float32)
    shared_piece = portion[slots_all:].reshape(
        tokens_here // packing, shards_in, packing, shared_units
    )
    shared_piece = shared_piece.transpose(0, 2, 1, 3).reshape(tokens_here, shards_in * shared_units)
    shared = jnp.dot(shared_piece, shared_down, preferred_element_type=jnp.float32)
    returned = lax.all_to_all(
        routed.astype(jnp.bfloat16).reshape(ep_size, capacity, columns),
        "ep",
        split_axis=0,
        concat_axis=0,
        tiled=True,
    )
    returned = returned.reshape(slots_all, columns)
    picked = jnp.take(returned, target, axis=0).reshape(tokens_here, TOP_K, columns)
    combined = shared + jnp.sum(route_weights[:, :, None] * picked.astype(jnp.float32), axis=1)
    return (attended, combined.astype(jnp.bfloat16))


def solution(mesh):
    placed = (
        P("ep", "tp"),
        P("ep", "tp"),
        P("ep", "tp"),
        P(),
        P(),
        P("tp"),
        P("ep", "tp"),
        P(),
        P("ep", None),
        P("ep", None),
        P("ep", None, "tp"),
        P("ep", None, "tp"),
        P("ep", None, "tp"),
        P(None, "tp"),
        P(None, "tp"),
        P(None, "tp"),
    )
    return jax.shard_map(
        shards,
        mesh=mesh,
        in_specs=placed,
        out_specs=(P("ep", "tp"), P("ep", "tp")),
        check_vma=False,
    )
```

profile of v0, /device:TPU:0, one launch (start us, length us, event | category | flops | bytes accessed | tf_op | source)
XLA Modules:
  0.0 298.6 jit_solution(4147302405466254535)
XLA Ops:
  7.2 0.9 copy.83
  8.3 1.4 reduce-window.6
  11.2 4.2 %gather_fusion = bf16[960,1024]{1,0:T(8,128)(2,1)S(1)} fusion(bf16[160,1024]{1,0:T(8,128)(2,1)S(1)} %copy-done.1, s32[1024]{0:T(1024)S(1)} %pad_clamp_fusion.1), kind=kCustom, calls=%fused_computation | custom fusion | bytes 3936000 | tf_op jit(solution)/shard_map/jit(_take)/gather | solution.py:138
  15.4 1.5 select_select_fusion
  16.9 6.4 %all-to-all-start = ((bf16[8,120,1024]{2,1,0:T(8,128)(2,1)}), bf16[8,120,1024]{2,1,0:T(8,128)(2,1)S(1)}, u32[]{:S(2)}, u32[]{:S(2)}) async-start(bf16[8,120,1024]{2,1,0:T(8,128)(2,1)} %select_select_fusion), calls=%async_computation | async-start | bytes 3932160 | tf_op jit(solution)/shard_map/all_to_all | solution.py:140
  23.3 0.7 all-gather.6.cloned.1.call-update
  24.0 45.4 %all-to-all-done = bf16[8,120,1024]{2,1,0:T(8,128)(2,1)S(1)} async-done(((bf16[8,120,1024]{2,1,0:T(8,128)(2,1)}), bf16[8,120,1024]{2,1,0:T(8,128)(2,1)S(1)}, u32[]{:S(2)}, u32[]{:S(2)}) %all-to-all-start) | async-done | bytes 1966112 | tf_op jit(solution)/shard_map/all_to_all | solution.py:140
  69.5 1.3 copy-done.6
  70.9 1.8 fusion.14
  72.8 2.1 fusion.37
  74.9 0.5 fusion.46
  75.4 77.6 %all-gather.4.cloned.1.call-done = bf16[960,4096]{1,0:T(8,128)(2,1)} async-done(((bf16[960,1024]{1,0:T(8,128)(2,1)}), bf16[960,4096]{1,0:T(8,128)(2,1)}) %all-gather.4.cloned.1.call-update) | async-done | bytes 7864336 | tf_op jit(solution)/shard_map/all_gather | solution.py:149
  153.1 5.0 %fusion.1 = f32[960]{0:T(1024)S(1)} fusion(bf16[960,4096]{1,0:T(8,128)(2,1)} %all-gather.4.cloned.1.call-done), kind=kLoop, calls=%fused_computation.5 | loop fusion | flops 11795520 | bytes 7868160 | tf_op jit(solution)/shard_map/reduce_sum | solution.py:91
  158.0 0.5 copy-done.5
  158.5 6.4 %fusion.3 = f32[960,512]{1,0:T(8,128)S(1)} fusion(bf16[960,4096]{1,0:T(8,128)(2,1)S(1)} %copy-done.5, f32[4096]{0:T(1024)S(1)} %copy-done.27, bf16[1,4096,512]{2,1,0:T(8,128)(2,1)} %param.27), kind=kOutput, calls=%fused_computation.9 | convolution fusion | flops 4038328320 | bytes 14041088 | tf_op jit(solution)/shard_map/dot_general | solution.py:90
  165.0 4.6 %multiply_convert_fusion = bf16[960,512]{1,0:T(8,128)(2,1)S(1)} fusion(f32[960,512]{1,0:T(8,128)S(1)} %fusion.3, bf16[1,4096,512]{2,1,0:T(8,128)(2,1)S(1)} %copy-done.25, bf16[960,4096]{1,0:T(8,128)(2,1)S(1)} %copy-done.5, f32[4096]{0:T(1024)S(1)} %copy-done.27, f32[960]{0:T(1024)S(1)} %add_rsqrt_fusion.2), kind=kOutput, calls=%fused_computation.33 | convolution fusion | flops 4042260480 | bytes 15027968 | tf_op jit(solution)/shard_map/dot_general | solution.py:89
  169.6 1.0 pad_maximum_fusion.1
  171.6 1.2 fusion.60
  174.1 1.0 pad_maximum_fusion.3
  175.1 1.3 collective-permute-start.1
  176.4 3.7 %collective-permute-start = (bf16[2,128,512]{1,2,0:T(8,128)(2,1)}, bf16[2,128,512]{1,2,0:T(8,128)(2,1)}, u32[]{:S(2)}, u32[]{:S(2)}) collective-permute-start(bf16[2,128,512]{1,2,0:T(8,128)(2,1)} %get-tuple-element.18), channel_id=1, source_target_pairs={{0,4},{4,8},{8,12},{12,16},{16,20},{20,24},{24,28},{1,5},{5,9},{9,... | collective-permute-start | bytes 786440 | tf_op jit(solution)/shard_map/ppermute | solution.py:20
  180.1 1.5 copy.75
  181.6 4.2 %reshape.381 = f32[512,4,2,128]{3,2,1,0:T(2,128)} reshape(bf16[512,1024]{1,0:T(8,128)(2,1)} %param.16) | data formatting | bytes 3145728 | tf_op jit(solution)/shard_map/convert_element_type | solution.py:34
  186.2 0.5 multiply_multiply_fusion
  187.0 2.0 copy.80
  189.0 1.9 copy.79
  190.9 1.9 copy.78
  192.8 1.9 copy.77
  194.8 0.6 add.209
  195.7 0.8 copy.88
  196.5 0.7 copy.90
  197.3 0.6 fusion.69
  197.9 1.4 fusion.30
  199.3 23.1 %all-gather.8.cloned.1.call-done = bf16[1000,2048]{1,0:T(8,128)(2,1)} async-done(((bf16[1000,512]{1,0:T(8,128)(2,1)}), bf16[1000,2048]{1,0:T(8,128)(2,1)}) %all-gather.8.cloned.1.call-update) | async-done | bytes 4096016 | tf_op jit(solution)/shard_map/all_gather | solution.py:164
  222.4 8.9 %fusion.20 = bf16[960,1024]{1,0:T(8,128)(2,1)} fusion(bf16[1,2048,1024]{2,1,0:T(8,128)(2,1)} %param.28, bf16[1000,2048]{1,0:T(8,128)(2,1)} %all-gather.8.cloned.1.call-done), kind=kOutput, calls=%fused_computation.35 | convolution fusion | flops 4027514880 | bytes 10092544 | tf_op jit(solution)/shard_map/dot_general | solution.py:166
  231.3 4.7 %all-to-all-start.1 = ((bf16[8,120,1024]{2,1,0:T(8,128)(2,1)}), bf16[8,120,1024]{2,1,0:T(8,128)(2,1)S(1)}, u32[]{:S(2)}, u32[]{:S(2)}) async-start(bf16[8,120,1024]{2,1,0:T(8,128)(2,1)} %bitcast.104), calls=%async_computation.1 | async-start | bytes 3932160 | tf_op jit(solution)/shard_map/all_to_all | solution.py:172
  236.0 1.3 pad_clamp_fusion
  237.3 1.5 pad_maximum_fusion
  239.2 0.6 copy-done.4
  239.8 0.9 copy-done.2
  240.7 7.2 %fusion.2 = (f32[4,2,512]{2,1,0:T(2,128)S(1)}, f32[4,768,512,2]{2,1,3,0:T(8,128)S(1)}) fusion(pred[512,768]{0,1:T(8,128)(4,1)} %fusion.30, bf16[768,4,128,1]{0,2,3,1:T(8,128)(2,1)S(1)} %bitcast.99, f32[512,4,2,32]{3,0,2,1:T(8,128)S(1)} %copy-done.2, f32[512,4,2,32]{3,0,2,1:T(8,128)S(1)} %copy-done.3, f32[512,4,2,32]{3,0,2,1:T(8,128)S(1)} %copy-done.4, ...), kind=kOutput, calls=%fused_computation.8 | convolution fusion | flops 819458048 | bytes 18514432 | tf_op jit(solution)/shard_map/qhgd,khd->hgqk/dot_general | solution.py:71
  248.0 4.2 %fusion.31 = bf16[4,128,2,512]{3,1,2,0:T(8,128)(2,1)} fusion(bf16[768,4,128,1]{0,2,3,1:T(8,128)(2,1)S(1)} %bitcast.106, f32[4,768,512,2]{2,1,3,0:T(8,128)S(1)} %get-tuple-element.29, f32[4,2,512]{2,1,0:T(2,128)S(1)} %broadcast_add_fusion, pred[512,768]{0,1:T(8,128)(4,1)S(1)} %copy-done.12), kind=kOutput, calls=%fused_computation.40 | convolution fusion | flops 818413568 | bytes 14827520 | tf_op jit(solution)/shard_map/hgqk,khd->qhgd/dot_general | solution.py:82
  252.2 2.3 copy.92
  254.7 27.6 %all-to-all-done.1 = bf16[8,120,1024]{2,1,0:T(8,128)(2,1)S(1)} async-done(((bf16[8,120,1024]{2,1,0:T(8,128)(2,1)}), bf16[8,120,1024]{2,1,0:T(8,128)(2,1)S(1)}, u32[]{:S(2)}, u32[]{:S(2)}) %all-to-all-start.1) | async-done | bytes 1966112 | tf_op jit(solution)/shard_map/all_to_all | solution.py:172
  282.2 3.5 %gather_fusion.1 = bf16[640,1024]{1,0:T(8,128)(2,1)} fusion(bf16[960,1024]{1,0:T(8,128)(2,1)S(1)} %bitcast.92, s32[1024]{0:T(1024)S(1)} %copy-done.19), kind=kCustom, calls=%fused_computation.1 | custom fusion | bytes 2624000 | tf_op jit(solution)/shard_map/jit(_take)/gather | solution.py:180
  285.7 2.6 gather.15
  288.4 2.6 multiply_reduce_fusion
  291.0 1.1 fusion.32
  (115 shorter events, 5.7 us)
Async XLA Ops:
  7.2 283.8 %copy-start = (bf16[512,1024]{1,0:T(8,128)(2,1)S(1)}, bf16[512,1024]{1,0:T(8,128)(2,1)}, u32[]{:S(2)}) copy-start(bf16[512,1024]{1,0:T(8,128)(2,1)} %param.31) | copy-start | bytes 3145732
  7.2 4.0 %copy-start.1 = (bf16[160,1024]{1,0:T(8,128)(2,1)S(1)}, bf16[160,1024]{1,0:T(8,128)(2,1)}, u32[]{:S(2)}) copy-start(bf16[160,1024]{1,0:T(8,128)(2,1)} %param.22) | copy-start | bytes 983044
  16.9 52.6 %all-to-all-start = ((bf16[8,120,1024]{2,1,0:T(8,128)(2,1)}), bf16[8,120,1024]{2,1,0:T(8,128)(2,1)S(1)}, u32[]{:S(2)}, u32[]{:S(2)}) async-start(bf16[8,120,1024]{2,1,0:T(8,128)(2,1)} %select_select_fusion), calls=%async_computation | async-start | bytes 3932160 | tf_op jit(solution)/shard_map/all_to_all | solution.py:140
  23.3 49.5 %copy-start.27 = (f32[4096]{0:T(1024)S(1)}, f32[4096]{0:T(1024)}, u32[]{:S(2)}) copy-start(f32[4096]{0:T(1024)} %param.23) | copy-start | bytes 49156
  23.3 47.7 %all-gather.6.cloned.1.call-start = ((), (), s32[]{:S(2)}) async-start(), calls=%async_computation.3 | async-start | bytes 1638400 | tf_op jit(solution)/shard_map/all_gather | solution.py:152
  24.0 129.1 %all-gather.4.cloned.1.call-start = ((), (), s32[]{:S(2)}) async-start(), calls=%async_computation.2 | async-start | bytes 9830400 | tf_op jit(solution)/shard_map/all_gather | solution.py:149
  69.5 1.3 copy-start.6
  70.8 4.0 %copy-start.26 = (bf16[4096,128]{1,0:T(8,128)(2,1)S(1)}, bf16[4096,128]{1,0:T(8,128)(2,1)}, u32[]{:S(2)}) copy-start(bf16[4096,128]{1,0:T(8,128)(2,1)} %param.30) | copy-start | bytes 3145732
  70.9 151.5 %all-gather.8.cloned.1.call-start = ((), (), s32[]{:S(2)}) async-start(), calls=%async_computation.4 | async-start | bytes 5120000 | tf_op jit(solution)/shard_map/all_gather | solution.py:164
  70.9 4.0 %copy-start.13 = (bf16[160,4096]{1,0:T(8,128)(2,1)S(1)}, bf16[160,4096]{1,0:T(8,128)(2,1)}, u32[]{:S(2)}) copy-start(bf16[160,4096]{1,0:T(8,128)(2,1)} %all-gather.6.cloned.1.call-done) | copy-start | bytes 3932164
  153.1 5.5 %copy-start.5 = (bf16[960,4096]{1,0:T(8,128)(2,1)S(1)}, bf16[960,4096]{1,0:T(8,128)(2,1)}, u32[]{:S(2)}) copy-start(bf16[960,4096]{1,0:T(8,128)(2,1)} %all-gather.4.cloned.1.call-done) | copy-start | bytes 23592964
  158.5 6.4 %copy-start.25 = (bf16[1,4096,512]{2,1,0:T(8,128)(2,1)S(1)}, bf16[1,4096,512]{2,1,0:T(8,128)(2,1)}, u32[]{:S(2)}) copy-start(bf16[1,4096,512]{2,1,0:T(8,128)(2,1)} %param.26) | copy-start | bytes 12582916
  169.5 1.2 copy-start.14
  169.6 1.6 copy-start.15
  171.1 3.0 %copy-start.7 = (bf16[512,512]{0,1:T(8,128)(2,1)}, bf16[512,512]{0,1:T(8,128)(2,1)S(1)}, u32[]{:S(2)}) copy-start(bf16[512,512]{0,1:T(8,128)(2,1)S(1)} %copy.74) | copy-start | bytes 1572868
  171.4 1.9 copy-start.24
  172.8 0.7 copy-start.10
  172.8 0.8 copy-start.11
  174.1 2.3 copy-start.9
  175.1 62.2 %collective-permute-start.1 = (bf16[2,128,512]{1,2,0:T(8,128)(2,1)}, bf16[2,128,512]{1,2,0:T(8,128)(2,1)}, u32[]{:S(2)}, u32[]{:S(2)}) collective-permute-start(bf16[2,128,512]{1,2,0:T(8,128)(2,1)} %get-tuple-element.19), channel_id=1, source_target_pairs={{4,0},{8,4},{12,8},{16,12},{20,16},{24,20},{28,24},{5,1},{9,5},{13... | collective-permute-start | bytes 786440 | tf_op jit(solution)/shard_map/ppermute | solution.py:23
  176.4 60.9 %collective-permute-start = (bf16[2,128,512]{1,2,0:T(8,128)(2,1)}, bf16[2,128,512]{1,2,0:T(8,128)(2,1)}, u32[]{:S(2)}, u32[]{:S(2)}) collective-permute-start(bf16[2,128,512]{1,2,0:T(8,128)(2,1)} %get-tuple-element.18), channel_id=1, source_target_pairs={{0,4},{4,8},{8,12},{12,16},{16,20},{20,24},{24,28},{1,5},{5,9},{9,... | collective-permute-start | bytes 786440 | tf_op jit(solution)/shard_map/ppermute | solution.py:20
  181.6 4.6 %copy-start.21 = (f32[128]{0:T(128)S(1)}, f32[128]{0:T(128)}, u32[]{:S(2)}) copy-start(f32[128]{0:T(128)} %param.19) | copy-start | bytes 1540
  190.9 3.9 %copy-start.28 = (f32[8]{0:T(128)S(1)}, f32[8]{0:T(128)}, u32[]{:S(2)}) copy-start(f32[8]{0:T(128)} %param.21) | copy-start | bytes 100
  190.9 4.5 %copy-start.18 = (s32[160,4]{0,1:T(4,128)S(1)}, s32[160,4]{0,1:T(4,128)}, u32[]{:S(2)}) copy-start(s32[160,4]{0,1:T(4,128)} %param.24) | copy-start | bytes 7684
  190.9 4.8 %copy-start.23 = (f32[160,4]{0,1:T(4,128)S(1)}, f32[160,4]{0,1:T(4,128)}, u32[]{:S(2)}) copy-start(f32[160,4]{0,1:T(4,128)} %param.25) | copy-start | bytes 7684
  231.3 6.0 %copy-start.8 = (bf16[512,512]{0,1:T(8,128)(2,1)S(1)}, bf16[512,512]{0,1:T(8,128)(2,1)}, u32[]{:S(2)}) copy-start(bf16[512,512]{0,1:T(8,128)(2,1)} %copy-done.7) | copy-start | bytes 1572868
  231.3 51.0 %all-to-all-start.1 = ((bf16[8,120,1024]{2,1,0:T(8,128)(2,1)}), bf16[8,120,1024]{2,1,0:T(8,128)(2,1)S(1)}, u32[]{:S(2)}, u32[]{:S(2)}) async-start(bf16[8,120,1024]{2,1,0:T(8,128)(2,1)} %bitcast.104), calls=%async_computation.1 | async-start | bytes 3932160 | tf_op jit(solution)/shard_map/all_to_all | solution.py:172
  237.3 1.9 copy-start.3
  237.3 2.5 copy-start.4
  238.8 1.9 copy-start.2
  238.8 1.9 copy-start.22
  240.7 7.2 %copy-start.20 = (f32[4,2]{1,0:T(4,128)S(1)}, f32[4,2]{1,0:T(4,128)}, u32[]{:S(2)}) copy-start(f32[4,2]{1,0:T(4,128)} %add.209) | copy-start | bytes 100
  240.7 7.3 %copy-start.12 = (pred[512,768]{0,1:T(8,128)(4,1)S(1)}, pred[512,768]{0,1:T(8,128)(4,1)}, u32[]{:S(2)}) copy-start(pred[512,768]{0,1:T(8,128)(4,1)} %fusion.30) | copy-start | bytes 1179652
  252.2 2.3 slice-start
  252.2 30.0 %copy-start.19 = (s32[1024]{0:T(1024)S(1)}, s32[1024]{0:T(1024)}, u32[]{:S(2)}) copy-start(s32[1024]{0:T(1024)} %pad_clamp_fusion) | copy-start | bytes 12292
  285.7 2.7 copy-start.16
  285.7 2.7 copy-start.17
Sparse Core Ops, SparseCore 0:
  25.9 30.1 all-gather.5
  71.0 82.0 all-gather.3
  170.7 51.6 all-gather.7
where the time goes:
time: 299 us
  waiting for transfers between devices  174 us (58%)
  local copies, waits for them, and re-layouts  35.3 us (12%)
  matrix products  34.9 us (12%)
  other arithmetic  23.4 us (8%)
  starting transfers between devices  16.2 us (5%)
  between operations  14.3 us (5%)
    all_gather x1, waiting for transfers between devices, shards(): lax.all_gather(arrived, 'tp', axis=1, tiled=True)  77.6 us
    all_to_all x1, waiting for transfers between devices, shards(): lax.all_to_all(outgoing.reshape(ep_size, capacity, width_here), 'ep', spl...  45.4 us
    all_to_all x1, waiting for transfers between devices, shards(): lax.all_to_all(routed.astype(jnp.bfloat16).reshape(ep_size, capacity, col...  27.6 us
    all_gather x1, waiting for transfers between devices, shards(): portion = lax.all_gather(stacked, 'tp', axis=1, tiled=True)  23.1 us
    dot_general x1, matrix products, shards(): jnp.dot(portion[:slots_all], local_down, preferred_element_type=jnp.float32)  8.88 us
    unnamed x63, local copies, waits for them, and re-layouts  8.45 us
    concatenate x4, local copies, waits for them, and re-layouts, rotate_heads(): jnp.concatenate([half_turn(row_half), half_turn(col_half)], axis=-1)  7.81 us
    dot_general x1, matrix products, attend_window(): jnp.einsum('qhgd,khd->hgqk', queries.reshape(length, kv_here, grouping, H...  7.16 us
  transfers between devices with their start and end apart: 7, of which 4 were waited for; matrix products, arithmetic and copies ran while one was open for 18% of the time, Pallas kernels for 0%

commit v1 on v0

--- a/solution.py
+++ b/solution.py
@@ -161,7 +161,8 @@
         [hidden, shared_hidden.reshape(tokens_here // packing, units_here)], axis=0
     )
     columns = local_down.shape[1]
-    portion = lax.all_gather(stacked, "tp", axis=1, tiled=True)
+    shards_2 = lax.all_gather(stacked, "tp")
+    portion = jnp.concatenate(shards_2, axis=1)
     shards_in = portion.shape[1] // units_here
     routed = jnp.dot(portion[:slots_all], local_down, preferred_element_type=jnp.float32)
     shared_piece = portion[slots_all:].reshape(

time: 299 us -> 304 us (1.017)
  local copies, waits for them, and re-layouts: 35.3 us -> 44.3 us
  matrix products: 34.9 us -> 31.5 us
    all_gather x0 -> x1, local copies, waits for them, and re-layouts: none -> 4.27 us  [shards(): shards_2 = lax.all_gather(stacked, 'tp')]
    dot_general x1, matrix products: 8.88 us -> 5.39 us  [shards(): jnp.dot(portion[:slots_all], local_down, preferred_element_type=jnp.float32)]
    unnamed x63 -> x68, local copies, waits for them, and re-layouts: 8.45 us -> 11.2 us
  transfers between devices with their start and end apart: 7 -> 7, of which waited for: 4 -> 4; matrix products, arithmetic and copies ran while one was open for 18% -> 19% of each run, Pallas kernels for 0% -> 0%
where the time goes in v1:
time: 304 us
  waiting for transfers between devices  174 us (57%)
  local copies, waits for them, and re-layouts  44.3 us (15%)
  matrix products  31.5 us (10%)
  other arithmetic  23.4 us (8%)
  starting transfers between devices  16.2 us (5%)
  between operations  14.4 us (5%)
    all_gather x1, waiting for transfers between devices, shards(): lax.all_gather(arrived, 'tp', axis=1, tiled=True)  77.6 us
    all_to_all x1, waiting for transfers between devices, shards(): lax.all_to_all(outgoing.reshape(ep_size, capacity, width_here), 'ep', spl...  45.4 us
    all_to_all x1, waiting for transfers between devices, shards(): lax.all_to_all(routed.astype(jnp.bfloat16).reshape(ep_size, capacity, col...  26.8 us
    all_gather x1, waiting for transfers between devices, shards(): shards_2 = lax.all_gather(stacked, 'tp')  23.2 us
    unnamed x68, local copies, waits for them, and re-layouts  11.2 us
    concatenate x4, local copies, waits for them, and re-layouts, rotate_heads(): jnp.concatenate([half_turn(row_half), half_turn(col_half)], axis=-1)  7.81 us
    dot_general x1, matrix products, attend_window(): jnp.einsum('qhgd,khd->hgqk', queries.reshape(length, kv_here, grouping, H...  7.16 us
    dot_general x2, matrix products, project(): up_sum = jnp.dot(weighted, up_rows, preferred_element_type=jnp.float32)  6.92 us
  transfers between devices with their start and end apart: 7, of which 4 were waited for; matrix products, arithmetic and copies ran while one was open for 19% of the time, Pallas kernels for 0%

profile of v1, /device:TPU:0, one launch (start us, length us, event | category | flops | bytes accessed | tf_op | source)
XLA Modules:
  0.0 303.6 jit_solution(5480694493810051660)
XLA Ops:
  7.2 0.9 copy.85
  8.3 1.4 reduce-window.6
  11.2 4.2 %gather_fusion = bf16[960,1024]{1,0:T(8,128)(2,1)S(1)} fusion(bf16[160,1024]{1,0:T(8,128)(2,1)S(1)} %copy-done.1, s32[1024]{0:T(1024)S(1)} %pad_clamp_fusion.1), kind=kCustom, calls=%fused_computation | custom fusion | bytes 3936000 | tf_op jit(solution)/shard_map/jit(_take)/gather | solution.py:138
  15.4 1.5 select_select_fusion
  16.9 6.4 %all-to-all-start = ((bf16[8,120,1024]{2,1,0:T(8,128)(2,1)}), bf16[8,120,1024]{2,1,0:T(8,128)(2,1)S(1)}, u32[]{:S(2)}, u32[]{:S(2)}) async-start(bf16[8,120,1024]{2,1,0:T(8,128)(2,1)} %select_select_fusion), calls=%async_computation | async-start | bytes 3932160 | tf_op jit(solution)/shard_map/all_to_all | solution.py:140
  23.3 0.7 all-gather.7.cloned.1.call-update
  24.0 45.4 %all-to-all-done = bf16[8,120,1024]{2,1,0:T(8,128)(2,1)S(1)} async-done(((bf16[8,120,1024]{2,1,0:T(8,128)(2,1)}), bf16[8,120,1024]{2,1,0:T(8,128)(2,1)S(1)}, u32[]{:S(2)}, u32[]{:S(2)}) %all-to-all-start) | async-done | bytes 1966112 | tf_op jit(solution)/shard_map/all_to_all | solution.py:140
  69.5 1.3 copy-done.7
  70.9 1.8 fusion.13
  72.8 2.1 fusion.34
  75.4 77.6 %all-gather.5.cloned.1.call-done = bf16[960,4096]{1,0:T(8,128)(2,1)} async-done(((bf16[960,1024]{1,0:T(8,128)(2,1)}), bf16[960,4096]{1,0:T(8,128)(2,1)}) %all-gather.5.cloned.1.call-update) | async-done | bytes 7864336 | tf_op jit(solution)/shard_map/all_gather | solution.py:149
  153.1 5.0 %fusion.1 = f32[960]{0:T(1024)S(1)} fusion(bf16[960,4096]{1,0:T(8,128)(2,1)} %all-gather.5.cloned.1.call-done), kind=kLoop, calls=%fused_computation.5 | loop fusion | flops 11795520 | bytes 7868160 | tf_op jit(solution)/shard_map/reduce_sum | solution.py:91
  158.5 6.4 %fusion.3 = f32[960,512]{1,0:T(8,128)S(1)} fusion(bf16[960,4096]{1,0:T(8,128)(2,1)S(1)} %copy-done.6, f32[4096]{0:T(1024)S(1)} %copy-done.29, bf16[1,4096,512]{2,1,0:T(8,128)(2,1)} %param.27), kind=kOutput, calls=%fused_computation.9 | convolution fusion | flops 4038328320 | bytes 14041088 | tf_op jit(solution)/shard_map/dot_general | solution.py:90
  165.0 4.6 %multiply_convert_fusion = bf16[960,512]{1,0:T(8,128)(2,1)S(1)} fusion(f32[960,512]{1,0:T(8,128)S(1)} %fusion.3, bf16[1,4096,512]{2,1,0:T(8,128)(2,1)S(1)} %copy-done.26, bf16[960,4096]{1,0:T(8,128)(2,1)S(1)} %copy-done.6, f32[4096]{0:T(1024)S(1)} %copy-done.29, f32[960]{0:T(1024)S(1)} %add_rsqrt_fusion.2), kind=kOutput, calls=%fused_computation.33 | convolution fusion | flops 4042260480 | bytes 15027968 | tf_op jit(solution)/shard_map/dot_general | solution.py:89
  169.6 1.0 pad_maximum_fusion.1
  171.6 1.2 fusion.57
  174.1 1.0 pad_maximum_fusion.3
  175.1 1.3 collective-permute-start.1
  176.4 3.7 %collective-permute-start = (bf16[2,128,512]{1,2,0:T(8,128)(2,1)}, bf16[2,128,512]{1,2,0:T(8,128)(2,1)}, u32[]{:S(2)}, u32[]{:S(2)}) collective-permute-start(bf16[2,128,512]{1,2,0:T(8,128)(2,1)} %get-tuple-element.18), channel_id=1, source_target_pairs={{0,4},{4,8},{8,12},{12,16},{16,20},{20,24},{24,28},{1,5},{5,9},{9,... | collective-permute-start | bytes 786440 | tf_op jit(solution)/shard_map/ppermute | solution.py:20
  180.1 1.5 copy.77
  181.6 4.1 %reshape.389 = f32[512,4,2,128]{3,2,1,0:T(2,128)} reshape(bf16[512,1024]{1,0:T(8,128)(2,1)} %param.16) | data formatting | bytes 3145728 | tf_op jit(solution)/shard_map/convert_element_type | solution.py:34
  186.9 2.0 copy.82
  188.9 1.9 copy.81
  190.9 1.9 copy.80
  192.8 1.9 copy.79
  194.8 0.6 add.209
  195.7 0.8 copy.91
  196.5 0.7 copy.93
  197.9 1.4 fusion.27
  199.3 23.2 %all-gather.9.cloned.1.call-done = bf16[4000,512]{1,0:T(8,128)(2,1)} async-done(((bf16[1000,512]{1,0:T(8,128)(2,1)}), bf16[4000,512]{1,0:T(8,128)(2,1)}) %all-gather.9.cloned.1.call-update) | async-done | bytes 4096016 | tf_op jit(solution)/shard_map/all_gather | solution.py:164
  222.5 4.3 %copy.118 = bf16[4,1000,512]{2,0,1:T(4,128)(2,1)S(1)} copy(bf16[4,1000,512]{2,1,0:T(8,128)(2,1)} %bitcast.111) | data formatting | bytes 8192000 | tf_op jit(solution)/shard_map/all_gather | solution.py:164
  226.8 1.4 slice.53
  228.7 1.3 copy.102
  230.0 0.9 copy-done.27
  230.9 5.4 %fusion.19 = bf16[960,1024]{1,0:T(8,128)(2,1)} fusion(bf16[960,2048]{1,0:T(8,128)(2,1)S(1)} %bitcast.112, bf16[1,2048,1024]{2,1,0:T(8,128)(2,1)S(1)} %copy-done.27), kind=kOutput, calls=%fused_computation.35 | convolution fusion | flops 4027514880 | bytes 10092544 | tf_op jit(solution)/shard_map/dot_general | solution.py:167
  236.3 4.7 %all-to-all-start.1 = ((bf16[8,120,1024]{2,1,0:T(8,128)(2,1)}), bf16[8,120,1024]{2,1,0:T(8,128)(2,1)S(1)}, u32[]{:S(2)}, u32[]{:S(2)}) async-start(bf16[8,120,1024]{2,1,0:T(8,128)(2,1)} %bitcast.118), calls=%async_computation.1 | async-start | bytes 3932160 | tf_op jit(solution)/shard_map/all_to_all | solution.py:173
  241.0 1.3 pad_clamp_fusion
  242.3 1.5 pad_maximum_fusion
  244.9 0.9 copy-done.3
  245.7 7.2 %fusion.2 = (f32[4,2,512]{2,1,0:T(2,128)S(1)}, f32[4,768,512,2]{2,1,3,0:T(8,128)S(1)}) fusion(pred[512,768]{0,1:T(8,128)(4,1)} %fusion.27, bf16[768,4,128,1]{0,2,3,1:T(8,128)(2,1)S(1)} %bitcast.113, f32[512,4,2,32]{3,0,2,1:T(8,128)S(1)} %copy-done.3, f32[512,4,2,32]{3,0,2,1:T(8,128)S(1)} %copy-done.4, f32[512,4,2,32]{3,0,2,1:T(8,128)S(1)} %copy-done.5, ...), kind=kOutput, calls=%fused_computation.8 | convolution fusion | flops 819458048 | bytes 18514432 | tf_op jit(solution)/shard_map/qhgd,khd->hgqk/dot_general | solution.py:71
  253.0 4.2 %fusion.28 = bf16[4,128,2,512]{3,1,2,0:T(8,128)(2,1)} fusion(bf16[768,4,128,1]{0,2,3,1:T(8,128)(2,1)S(1)} %bitcast.120, f32[4,768,512,2]{2,1,3,0:T(8,128)S(1)} %get-tuple-element.29, f32[4,2,512]{2,1,0:T(2,128)S(1)} %broadcast_add_fusion, pred[512,768]{0,1:T(8,128)(4,1)S(1)} %copy-done.13), kind=kOutput, calls=%fused_computation.40 | convolution fusion | flops 818413568 | bytes 14827520 | tf_op jit(solution)/shard_map/hgqk,khd->qhgd/dot_general | solution.py:82
  257.2 2.3 copy.95
  259.5 1.0 slice.52
  260.5 26.8 %all-to-all-done.1 = bf16[8,120,1024]{2,1,0:T(8,128)(2,1)S(1)} async-done(((bf16[8,120,1024]{2,1,0:T(8,128)(2,1)}), bf16[8,120,1024]{2,1,0:T(8,128)(2,1)S(1)}, u32[]{:S(2)}, u32[]{:S(2)}) %all-to-all-start.1) | async-done | bytes 1966112 | tf_op jit(solution)/shard_map/all_to_all | solution.py:173
  287.3 3.5 %gather_fusion.1 = bf16[640,1024]{1,0:T(8,128)(2,1)} fusion(bf16[960,1024]{1,0:T(8,128)(2,1)S(1)} %bitcast.101, s32[1024]{0:T(1024)S(1)} %copy-done.20), kind=kCustom, calls=%fused_computation.1 | custom fusion | bytes 2624000 | tf_op jit(solution)/shard_map/jit(_take)/gather | solution.py:181
  290.7 2.6 gather.15
  293.4 2.6 multiply_reduce_fusion
  296.0 1.1 fusion.29
  (119 shorter events, 8.8 us)
Async XLA Ops:
  7.2 288.8 %copy-start = (bf16[512,1024]{1,0:T(8,128)(2,1)S(1)}, bf16[512,1024]{1,0:T(8,128)(2,1)}, u32[]{:S(2)}) copy-start(bf16[512,1024]{1,0:T(8,128)(2,1)} %param.31) | copy-start | bytes 3145732
  7.2 4.0 %copy-start.1 = (bf16[160,1024]{1,0:T(8,128)(2,1)S(1)}, bf16[160,1024]{1,0:T(8,128)(2,1)}, u32[]{:S(2)}) copy-start(bf16[160,1024]{1,0:T(8,128)(2,1)} %param.22) | copy-start | bytes 983044
  16.9 52.6 %all-to-all-start = ((bf16[8,120,1024]{2,1,0:T(8,128)(2,1)}), bf16[8,120,1024]{2,1,0:T(8,128)(2,1)S(1)}, u32[]{:S(2)}, u32[]{:S(2)}) async-start(bf16[8,120,1024]{2,1,0:T(8,128)(2,1)} %select_select_fusion), calls=%async_computation | async-start | bytes 3932160 | tf_op jit(solution)/shard_map/all_to_all | solution.py:140
  23.3 49.5 %copy-start.29 = (f32[4096]{0:T(1024)S(1)}, f32[4096]{0:T(1024)}, u32[]{:S(2)}) copy-start(f32[4096]{0:T(1024)} %param.23) | copy-start | bytes 49156
  23.3 47.7 %all-gather.7.cloned.1.call-start = ((), (), s32[]{:S(2)}) async-start(), calls=%async_computation.3 | async-start | bytes 1638400 | tf_op jit(solution)/shard_map/all_gather | solution.py:152
  24.0 129.1 %all-gather.5.cloned.1.call-start = ((), (), s32[]{:S(2)}) async-start(), calls=%async_computation.2 | async-start | bytes 9830400 | tf_op jit(solution)/shard_map/all_gather | solution.py:149
  69.5 1.3 copy-start.7
  70.8 4.0 %copy-start.28 = (bf16[4096,128]{1,0:T(8,128)(2,1)S(1)}, bf16[4096,128]{1,0:T(8,128)(2,1)}, u32[]{:S(2)}) copy-start(bf16[4096,128]{1,0:T(8,128)(2,1)} %param.30) | copy-start | bytes 3145732
  70.9 151.7 %all-gather.9.cloned.1.call-start = ((), (), s32[]{:S(2)}) async-start(), calls=%async_computation.4 | async-start | bytes 5120000 | tf_op jit(solution)/shard_map/all_gather | solution.py:164
  70.9 4.0 %copy-start.14 = (bf16[160,4096]{1,0:T(8,128)(2,1)S(1)}, bf16[160,4096]{1,0:T(8,128)(2,1)}, u32[]{:S(2)}) copy-start(bf16[160,4096]{1,0:T(8,128)(2,1)} %all-gather.7.cloned.1.call-done) | copy-start | bytes 3932164
  153.1 5.5 %copy-start.6 = (bf16[960,4096]{1,0:T(8,128)(2,1)S(1)}, bf16[960,4096]{1,0:T(8,128)(2,1)}, u32[]{:S(2)}) copy-start(bf16[960,4096]{1,0:T(8,128)(2,1)} %all-gather.5.cloned.1.call-done) | copy-start | bytes 23592964
  158.5 6.4 %copy-start.26 = (bf16[1,4096,512]{2,1,0:T(8,128)(2,1)S(1)}, bf16[1,4096,512]{2,1,0:T(8,128)(2,1)}, u32[]{:S(2)}) copy-start(bf16[1,4096,512]{2,1,0:T(8,128)(2,1)} %param.26) | copy-start | bytes 12582916
  169.5 1.2 copy-start.15
  169.6 1.6 copy-start.16
  171.1 3.0 copy-start.8
  171.4 1.9 copy-start.25
  172.8 0.7 copy-start.11
  172.8 0.8 copy-start.12
  174.1 2.3 copy-start.10
  175.1 67.2 %collective-permute-start.1 = (bf16[2,128,512]{1,2,0:T(8,128)(2,1)}, bf16[2,128,512]{1,2,0:T(8,128)(2,1)}, u32[]{:S(2)}, u32[]{:S(2)}) collective-permute-start(bf16[2,128,512]{1,2,0:T(8,128)(2,1)} %get-tuple-element.19), channel_id=1, source_target_pairs={{4,0},{8,4},{12,8},{16,12},{20,16},{24,20},{28,24},{5,1},{9,5},{13... | collective-permute-start | bytes 786440 | tf_op jit(solution)/shard_map/ppermute | solution.py:23
  176.4 66.0 %collective-permute-start = (bf16[2,128,512]{1,2,0:T(8,128)(2,1)}, bf16[2,128,512]{1,2,0:T(8,128)(2,1)}, u32[]{:S(2)}, u32[]{:S(2)}) collective-permute-start(bf16[2,128,512]{1,2,0:T(8,128)(2,1)} %get-tuple-element.18), channel_id=1, source_target_pairs={{0,4},{4,8},{8,12},{12,16},{16,20},{20,24},{24,28},{1,5},{5,9},{9,... | collective-permute-start | bytes 786440 | tf_op jit(solution)/shard_map/ppermute | solution.py:20
  181.6 4.6 %copy-start.22 = (f32[128]{0:T(128)S(1)}, f32[128]{0:T(128)}, u32[]{:S(2)}) copy-start(f32[128]{0:T(128)} %param.19) | copy-start | bytes 1540
  190.9 3.9 %copy-start.30 = (f32[8]{0:T(128)S(1)}, f32[8]{0:T(128)}, u32[]{:S(2)}) copy-start(f32[8]{0:T(128)} %param.21) | copy-start | bytes 100
  190.9 4.5 %copy-start.19 = (s32[160,4]{0,1:T(4,128)S(1)}, s32[160,4]{0,1:T(4,128)}, u32[]{:S(2)}) copy-start(s32[160,4]{0,1:T(4,128)} %param.24) | copy-start | bytes 7684
  190.9 4.8 %copy-start.24 = (f32[160,4]{0,1:T(4,128)S(1)}, f32[160,4]{0,1:T(4,128)}, u32[]{:S(2)}) copy-start(f32[160,4]{0,1:T(4,128)} %param.25) | copy-start | bytes 7684
  226.8 1.9 copy-start.2
  228.7 2.2 copy-start.27
  236.3 6.0 %copy-start.9 = (bf16[512,512]{0,1:T(8,128)(2,1)S(1)}, bf16[512,512]{0,1:T(8,128)(2,1)}, u32[]{:S(2)}) copy-start(bf16[512,512]{0,1:T(8,128)(2,1)} %copy-done.8) | copy-start | bytes 1572868
  236.3 51.0 %all-to-all-start.1 = ((bf16[8,120,1024]{2,1,0:T(8,128)(2,1)}), bf16[8,120,1024]{2,1,0:T(8,128)(2,1)S(1)}, u32[]{:S(2)}, u32[]{:S(2)}) async-start(bf16[8,120,1024]{2,1,0:T(8,128)(2,1)} %bitcast.118), calls=%async_computation.1 | async-start | bytes 3932160 | tf_op jit(solution)/shard_map/all_to_all | solution.py:173
  242.3 1.9 copy-start.4
  242.3 2.5 copy-start.5
  243.8 1.9 copy-start.3
  243.8 1.9 copy-start.23
  245.7 7.2 %copy-start.21 = (f32[4,2]{1,0:T(4,128)S(1)}, f32[4,2]{1,0:T(4,128)}, u32[]{:S(2)}) copy-start(f32[4,2]{1,0:T(4,128)} %add.209) | copy-start | bytes 100
  245.7 7.3 %copy-start.13 = (pred[512,768]{0,1:T(8,128)(4,1)S(1)}, pred[512,768]{0,1:T(8,128)(4,1)}, u32[]{:S(2)}) copy-start(pred[512,768]{0,1:T(8,128)(4,1)} %fusion.27) | copy-start | bytes 1179652
  257.2 30.0 %copy-start.20 = (s32[1024]{0:T(1024)S(1)}, s32[1024]{0:T(1024)}, u32[]{:S(2)}) copy-start(s32[1024]{0:T(1024)} %pad_clamp_fusion) | copy-start | bytes 12292
  290.7 2.7 copy-start.17
  290.7 2.7 copy-start.18
Sparse Core Ops, SparseCore 0:
  25.9 30.1 all-gather.6
  71.0 82.0 all-gather.4
  170.7 51.7 all-gather.8
